TPU v7x, 32 devices: a whole 2x2x4 slice. The times are simulated.
32 devices in a mesh: fs: 8 (over z, core), tp: 4 (over y, x).
Axes of the slice: x: 2, y: 2, z: 4, core: 2. Of those that a mesh axis runs over, the one named last changes fastest.
Arguments:
- rows_later: bfloat16 [6144, 2048], P('fs'), may hold values from -6 to 6
- rows_earlier: bfloat16 [6144, 2048], P('fs'), may hold values from -6 to 6
- out_cotangent: bfloat16 [6144, 4096], P('fs', 'tp'), may hold values from -6 to 6
- gate_proj: bfloat16 [2048, 4096], P('fs', 'tp'), may hold values from -0.125 to 0.125
- up_proj: bfloat16 [2048, 4096], P('fs', 'tp'), may hold values from -0.125 to 0.125
- conv_taps: float32 [3, 4096], P(None, 'tp'), may hold values from -4 to 4
- conv_bias: float32 [4096], P('tp'), may hold values from -3 to 3
- gate_grad_sum: float32 [2048, 4096], P('fs', 'tp'), may hold values from -6 to 6
- up_grad_sum: float32 [2048, 4096], P('fs', 'tp'), may hold values from -6 to 6
- taps_grad_sum: float32 [3, 4096], P(None, 'tp'), may hold values from -6 to 6
- bias_grad_sum: float32 [4096], P('tp'), may hold values from -6 to 6
Outputs:
- hidden_later: bfloat16 [6144, 4096], P('fs', 'tp')
- input_grad: bfloat16 [6144, 2048], P('fs')
- gate_grad_out: float32 [2048, 4096], P('fs', 'tp')
- up_grad_out: float32 [2048, 4096], P('fs', 'tp')
- taps_grad_out: float32 [3, 4096], P(None, 'tp')
- bias_grad_out: float32 [4096], P('tp')
All inputs are finite; a program needn't handle non-finite values.
Results may differ from a plain program's by a relative error of at most 0.019.
Values may be sent and summed in bfloat16 or wider, within the bound.
No kernel may reach another device: no remote copies, remote signals or barrier semaphores. Data moves between devices by JAX's collectives and lax.ppermute only.
A program may use at most 128 MiB of HBM per device.

v0:
```python
import jax
import jax.numpy as jnp
from jax import lax
from jax.sharding import PartitionSpec as P


def shift_down(values, distance):
    total_len = values.shape[1]
    return jnp.pad(values, ((0, 0), (distance, 0), (0, 0)))[:, :total_len]


def shift_up(values, distance):
    return jnp.pad(values, ((0, 0), (0, distance), (0, 0)))[:, distance:]


def causal_mix(pre_values, conv_taps, conv_bias):
    return (
        conv_taps[0] * shift_down(pre_values, 2)
        + conv_taps[1] * shift_down(pre_values, 1)
        + conv_taps[2] * pre_values
        + conv_bias
    )


def mix_adjoint(mixed_grad, conv_taps):
    return (
        conv_taps[2] * mixed_grad
        + conv_taps[1] * shift_up(mixed_grad, 1)
        + conv_taps[0] * shift_up(mixed_grad, 2)
    )


def contract_last(left, right):
    return lax.dot_general(
        left, right, (((1,), (1,)), ((), ())), preferred_element_type=jnp.float32
    )


def contract_first(left, right):
    return lax.dot_general(
        left, right, (((0,), (0,)), ((), ())), preferred_element_type=jnp.float32
    )


def on_device(
    rows_later,
    rows_earlier,
    out_cotangent,
    gate_proj,
    up_proj,
    conv_taps,
    conv_bias,
    gate_grad_sum,
    up_grad_sum,
    taps_grad_sum,
    bias_grad_sum,
):
    seq_len = rows_later.shape[0]
    shard_width = out_cotangent.shape[1]
    stacked_rows = jnp.concatenate([rows_later, rows_earlier], axis=0)
    paired = jnp.stack([gate_proj, up_proj], axis=0)
    pieces = lax.all_gather(paired, "fs", axis=1, tiled=True)
    gate_acc = jnp.dot(stacked_rows, pieces[0], preferred_element_type=jnp.float32)
    up_acc = jnp.dot(stacked_rows, pieces[1], preferred_element_type=jnp.float32)
    gate_pre = gate_acc.astype(jnp.bfloat16)
    up_value = up_acc.astype(jnp.bfloat16)
    gate_pre, up_value = lax.optimization_barrier((gate_pre, up_value))
    gate_float = gate_pre.astype(jnp.float32).reshape(2, seq_len, shard_width)
    up_float = up_value.astype(jnp.float32).reshape(2, seq_len, shard_width)
    mixed = causal_mix(gate_float, conv_taps, conv_bias)
    sig_all = jax.nn.sigmoid(mixed)
    activated = mixed * sig_all
    hidden = (activated * up_float).astype(jnp.bfloat16)
    hidden_later = hidden[0]
    grad_scale = lax.rsqrt(jnp.asarray(seq_len * lax.axis_size("fs"), jnp.float32))

    def make_term(grad_rows):
        return contract_first(rows_earlier, grad_rows)

    cotangent = out_cotangent.astype(jnp.float32)[None]
    mixed_back = mixed[1:]
    sig_back = sig_all[1:]
    up_grad = (cotangent * activated[1:]).astype(jnp.bfloat16)[0]
    up_summed = lax.psum_scatter(
        make_term(up_grad).astype(jnp.bfloat16), "fs", scatter_dimension=0, tiled=True
    ).astype(jnp.float32)
    mixed_grad = cotangent * up_float[1:] * sig_back * (1.0 + mixed_back * (1.0 - sig_back))
    gate_grad = mix_adjoint(mixed_grad, conv_taps).astype(jnp.bfloat16)[0]
    gate_summed = lax.psum_scatter(
        make_term(gate_grad).astype(jnp.bfloat16), "fs", scatter_dimension=0, tiled=True
    ).astype(jnp.float32)
    pieces = lax.all_gather(paired, "fs", axis=1, tiled=True)
    partial_rows = contract_last(gate_grad, pieces[0]) + contract_last(up_grad, pieces[1])
    input_grad = lax.psum(partial_rows.astype(jnp.bfloat16), "tp")
    gate_grad_out = gate_grad_sum + grad_scale * gate_summed
    up_grad_out = up_grad_sum + grad_scale * up_summed
    gate_back = gate_float[1:]
    tap_local = jnp.stack(
        [
            jnp.sum(mixed_grad * shift_down(gate_back, 2 - tap_index), axis=(0, 1))
            for tap_index in range(conv_taps.shape[0])
        ]
    )
    bias_local = jnp.sum(mixed_grad, axis=(0, 1))
    tap_total, bias_total = lax.psum((tap_local, bias_local), "fs")
    taps_grad_out = taps_grad_sum + grad_scale * tap_total
    bias_grad_out = bias_grad_sum + grad_scale * bias_total
    return (hidden_later, input_grad, gate_grad_out, up_grad_out, taps_grad_out, bias_grad_out)


def solution(mesh):
    placed = (
        P("fs", None),
        P("fs", None),
        P("fs", "tp"),
        P("fs", "tp"),
        P("fs", "tp"),
        P(None, "tp"),
        P("tp"),
        P("fs", "tp"),
        P("fs", "tp"),
        P(None, "tp"),
        P("tp"),
    )
    return jax.shard_map(
        on_device,
        mesh=mesh,
        in_specs=placed,
        out_specs=(
            P("fs", "tp"),
            P("fs", None),
            P("fs", "tp"),
            P("fs", "tp"),
            P(None, "tp"),
            P("tp"),
        ),
        check_vma=False,
    )
```

profile of v0, /device:TPU:0, one launch (start us, length us, event | category | flops | bytes accessed | tf_op | source)
XLA Modules:
  0.0 333.8 jit_solution(14247439538161545756)
XLA Ops:
  7.2 0.0 all-gather.2.cloned.1.call-start
  7.2 2.4 pad_maximum_fusion
  9.6 0.0 all-gather.2.cloned.1.call-update
  9.7 0.0 reduce-scatter.3.cloned.1.call-start
  9.7 0.0 copy-start.5
  9.7 0.9 fusion.32
  10.7 2.0 constant_dynamic-update-slice_fusion.1
  12.6 2.1 constant_dynamic-update-slice_fusion
  14.8 80.2 %all-gather.2.cloned.1.call-done = bf16[2,2048,1024]{2,1,0:T(8,128)(2,1)} async-done(((bf16[2,256,1024]{2,1,0:T(8,128)(2,1)}), bf16[2,2048,1024]{2,1,0:T(8,128)(2,1)}) %all-gather.2.cloned.1.call-update) | async-done | bytes 8388624 | tf_op jit(solution)/shard_map/all_gather | solution.py:62
  95.0 10.1 %convolution_convert_fusion = bf16[1536,1024]{1,0:T(8,128)(2,1)S(1)} fusion(bf16[1536,2048]{1,0:T(8,128)(2,1)} %constant_dynamic-update-slice_fusion, bf16[2,2048,1024]{2,1,0:T(8,128)(2,1)} %all-gather.2.cloned.1.call-done), kind=kOutput, calls=%fused_computation.15 | convolution fusion | flops 6444023808 | bytes 13631488 | tf_op jit(solution)/shard_map/dot_general | solution.py:64
  105.1 8.8 %convolution_convert_fusion.1 = bf16[1536,1024]{1,0:T(8,128)(2,1)S(1)} fusion(bf16[1536,2048]{1,0:T(8,128)(2,1)} %constant_dynamic-update-slice_fusion, bf16[2,2048,1024]{2,1,0:T(8,128)(2,1)S(1)} %copy-done.15), kind=kOutput, calls=%fused_computation.16 | convolution fusion | flops 6444023808 | bytes 13631488 | tf_op jit(solution)/shard_map/dot_general | solution.py:63
  113.9 0.7 convert_element_type.59
  114.7 1.9 slice_bitcast_fusion.6
  116.5 0.7 convert_element_type.60
  117.3 3.2 add_divide_fusion
  120.5 0.6 copy-done.1
  121.1 6.3 %fusion.13 = (f32[1024]{0:T(1024)S(1)}, f32[1024]{0:T(1024)S(1)}, f32[1024]{0:T(1024)S(1)}, f32[1024]{0:T(1024)S(1)}, f32[1,768,1024]{2,1,0:T(8,128)S(1)}) fusion(f32[1,768,1024]{2,1,0:T(8,128)} %slice_bitcast_fusion.6, f32[1536,1024]{1,0:T(8,128)S(1)} %convert_element_type.59, f32[2,768,1024]{2,1,0:T(8,128)S(1)} %get-tuple-element.24, ...), kind=kLoop, calls=%fused_computation.29 | loop fusion | flops 11005952 | bytes 20463616 | tf_op jit(solution)/shard_map/reduce_sum | solution.py:100
  127.4 0.0 copy-start.6
  127.4 1.0 fusion.10
  128.4 0.0 copy-start.9
  128.4 1.1 copy-done.9
  129.5 5.1 %convert_bitcast_fusion.1 = bf16[2048,1024]{0,1:T(8,128)(2,1)} fusion(bf16[768,2048]{1,0:T(8,128)(2,1)S(1)} %copy-done.6, bf16[1,768,1024]{2,1,0:T(8,128)(2,1)S(1)} %fusion.10), kind=kOutput, calls=%fused_computation.12 | convolution fusion | flops 3223322624 | bytes 8912896 | tf_op jit(solution)/shard_map/dot_general | solution.py:40
  134.6 0.0 reduce-scatter.3.cloned.1.call-update
  134.6 0.2 reduce-scatter.5.cloned.1.call-start
  134.9 4.5 %fusion.29 = f32[2,768,1024]{2,1,0:T(8,128)S(1)} fusion(f32[2,768,1024]{2,1,0:T(8,128)} %copy-done), kind=kLoop, calls=%fused_computation.55 | loop fusion | flops 6291456 | bytes 12582912 | tf_op jit(solution)/shard_map/mul | solution.py:72
  139.4 2.6 copy-done.2
  142.0 5.1 %convert_bitcast_fusion = bf16[2048,1024]{0,1:T(8,128)(2,1)} fusion(bf16[768,2048]{1,0:T(8,128)(2,1)S(1)} %copy-done.6, f32[2,768,1024]{2,1,0:T(8,128)S(1)} %fusion.29, bf16[768,1024]{1,0:T(8,128)(2,1)S(1)} %copy-done.7), kind=kOutput, calls=%fused_computation.11 | convolution fusion | flops 3225681920 | bytes 12058624 | tf_op jit(solution)/shard_map/dot_general | solution.py:40
  147.1 0.0 reduce-scatter.5.cloned.1.call-update
  147.2 0.0 copy-start.8
  147.2 0.0 all-reduce.9.cloned.1.call-start
  147.2 1.3 copy-done.10
  148.6 5.5 %fusion.5 = f32[768,2048]{1,0:T(8,128)S(1)} fusion(bf16[2,2048,1024]{2,1,0:T(8,128)(2,1)} %all-gather.2.cloned.1.call-done, bf16[1,768,1024]{2,1,0:T(8,128)(2,1)S(1)} %copy-done.10), kind=kOutput, calls=%fused_computation.17 | convolution fusion | flops 3221225472 | bytes 12058624 | tf_op jit(solution)/shard_map/dot_general | solution.py:34
  154.1 0.0 copy-start.11
  154.1 7.3 %add_convert_fusion = bf16[768,2048]{1,0:T(8,128)(2,1)} fusion(f32[768,2048]{1,0:T(8,128)S(1)} %fusion.5, bf16[2,2048,1024]{2,1,0:T(8,128)(2,1)} %all-gather.2.cloned.1.call-done, f32[2,768,1024]{2,1,0:T(8,128)S(1)} %copy-done.3, bf16[768,1024]{1,0:T(8,128)(2,1)S(1)} %copy-done.8), kind=kOutput, calls=%fused_computation.7 | convolution fusion | flops 3226730496 | bytes 18350080 | tf_op jit(solution)/shard_map/dot_general | solution.py:34
  161.4 0.0 all-reduce.9.cloned.1.call-update
  161.4 0.3 copy.17
  161.8 1.6 copy.18
  163.4 27.1 %all-reduce.6 = (f32[3,1024]{1,0:T(4,128)S(1)}, f32[1024]{0:T(1024)S(1)}) all-reduce(f32[3,1024]{1,0:T(4,128)S(1)} %pad_maximum_fusion.1, f32[1024]{0:T(1024)S(1)} %get-tuple-element.18), channel_id=1, replica_groups=mesh['fs'=8,'tp'=4] {'fs'}, use_global_device_ids=true, to_apply=%region_6.7 | all-reduce | flops 4096 | bytes 32768 | tf_op jit(solution)/shard_map/psum | solution.py:105
  190.5 0.6 multiply_add_fusion.3
  191.1 0.6 multiply_add_fusion.2
  191.7 4.5 %fusion.23 = bf16[768,1024]{1,0:T(8,128)(2,1)} fusion(f32[2,768,1024]{2,1,0:T(8,128)} %bitcast.61, f32[2,768,1024]{2,1,0:T(8,128)} %copy-done.2), kind=kLoop, calls=%fused_computation.43 | loop fusion | flops 1572864 | bytes 7864320 | tf_op jit(solution)/shard_map/squeeze | solution.py:74
  196.2 1.2 multiply_add_fusion.1
  197.4 1.3 copy.19
  198.7 35.6 %reduce-scatter.5.cloned.1.call-done = bf16[256,1024]{0,1:T(8,128)(2,1)} async-done(((bf16[2048,1024]{0,1:T(8,128)(2,1)}), bf16[256,1024]{0,1:T(8,128)(2,1)}) %reduce-scatter.5.cloned.1.call-update) | async-done | bytes 524304 | tf_op jit(solution)/shard_map/reduce_scatter | solution.py:84
  234.3 1.2 multiply_add_fusion
  235.5 1.3 copy.20
  236.8 86.5 %all-reduce.9.cloned.1.call-done = bf16[768,2048]{1,0:T(8,128)(2,1)} async-done(((bf16[768,2048]{1,0:T(8,128)(2,1)}), bf16[768,2048]{1,0:T(8,128)(2,1)}) %all-reduce.9.cloned.1.call-update) | async-done | bytes 3145744 | tf_op jit(solution)/shard_map/psum | solution.py:94
  323.3 4.0 %copy.23 = bf16[768,2048]{1,0:T(8,128)(2,1)} copy(bf16[768,2048]{1,0:T(8,128)(2,1)} %all-reduce.9.cloned.1.call-done) | data formatting | bytes 6291456
  (25 shorter events, 0.1 us)
Async XLA Ops:
  7.2 3.5 %copy-start.4 = (bf16[768,2048]{1,0:T(8,128)(2,1)S(1)}, bf16[768,2048]{1,0:T(8,128)(2,1)}, u32[]{:S(2)}) copy-start(bf16[768,2048]{1,0:T(8,128)(2,1)} %param.11) | copy-start | bytes 9437188
  7.2 87.8 %all-gather.2.cloned.1.call-start = ((), (), s32[]{:S(2)}) async-start(), calls=%async_computation.2 | async-start | bytes 9437184 | tf_op jit(solution)/shard_map/all_gather | solution.py:62
  9.7 186.6 %reduce-scatter.3.cloned.1.call-start = ((), (), s32[]{:S(2)}) async-start(), calls=%async_computation.4 | async-start | bytes 4718592 | tf_op jit(solution)/shard_map/reduce_scatter | solution.py:89
  9.7 2.9 copy-start.5
  95.0 10.1 %copy-start.15 = (bf16[2,2048,1024]{2,1,0:T(8,128)(2,1)S(1)}, bf16[2,2048,1024]{2,1,0:T(8,128)(2,1)}, u32[]{:S(2)}) copy-start(bf16[2,2048,1024]{2,1,0:T(8,128)(2,1)} %all-gather.2.cloned.1.call-done) | copy-start | bytes 25165828
  116.5 0.7 copy-start.14
  117.3 3.8 %copy-start.1 = (f32[1536,1024]{1,0:T(8,128)}, f32[1536,1024]{1,0:T(8,128)S(1)}, u32[]{:S(2)}) copy-start(f32[1536,1024]{1,0:T(8,128)S(1)} %convert_element_type.60) | copy-start | bytes 18874372
  120.5 6.9 %copy-start = (f32[2,768,1024]{2,1,0:T(8,128)}, f32[2,768,1024]{2,1,0:T(8,128)S(1)}, u32[]{:S(2)}) copy-start(f32[2,768,1024]{2,1,0:T(8,128)S(1)} %get-tuple-element.24) | copy-start | bytes 18874372
  127.4 2.2 copy-start.6
  128.4 1.1 copy-start.9
  134.6 99.7 %reduce-scatter.5.cloned.1.call-start = ((), (), s32[]{:S(2)}) async-start(), calls=%async_computation.5 | async-start | bytes 4718592 | tf_op jit(solution)/shard_map/reduce_scatter | solution.py:84
  134.9 7.1 %copy-start.7 = (bf16[768,1024]{1,0:T(8,128)(2,1)S(1)}, bf16[768,1024]{1,0:T(8,128)(2,1)}, u32[]{:S(2)}) copy-start(bf16[768,1024]{1,0:T(8,128)(2,1)} %param.13) | copy-start | bytes 4718596
  139.4 2.6 copy-start.2
  147.1 1.4 copy-start.10
  147.2 6.9 %copy-start.8 = (bf16[768,1024]{1,0:T(8,128)(2,1)S(1)}, bf16[768,1024]{1,0:T(8,128)(2,1)}, u32[]{:S(2)}) copy-start(bf16[768,1024]{1,0:T(8,128)(2,1)} %param.13) | copy-start | bytes 4718596
  147.2 176.1 %all-reduce.9.cloned.1.call-start = ((), (), s32[]{:S(2)}) async-start(), calls=%async_computation.3 | async-start | bytes 6291456 | tf_op jit(solution)/shard_map/psum | solution.py:94
  148.6 5.5 %copy-start.3 = (f32[2,768,1024]{2,1,0:T(8,128)S(1)}, f32[2,768,1024]{2,1,0:T(8,128)}, u32[]{:S(2)}) copy-start(f32[2,768,1024]{2,1,0:T(8,128)} %copy-done.2) | copy-start | bytes 18874372
  154.1 7.4 %copy-start.11 = (f32[256,1024]{1,0:T(8,128)S(1)}, f32[256,1024]{1,0:T(8,128)}, u32[]{:S(2)}) copy-start(f32[256,1024]{1,0:T(8,128)} %param.18) | copy-start | bytes 3145732
  161.4 29.1 %copy-start.13 = (f32[1024]{0:T(1024)S(1)}, f32[1024]{0:T(1024)}, u32[]{:S(2)}) copy-start(f32[1024]{0:T(1024)} %param.21) | copy-start | bytes 12292
  161.4 29.7 %copy-start.12 = (f32[3,1024]{1,0:T(4,128)S(1)}, f32[3,1024]{1,0:T(4,128)}, u32[]{:S(2)}) copy-start(f32[3,1024]{1,0:T(4,128)} %param.20) | copy-start | bytes 36868
Sparse Core Ops, SparseCore 0:
  10.2 84.7 all-gather.1
  134.8 48.8 reduce-scatter.2
  185.9 48.3 reduce-scatter.4
  237.9 85.4 all-reduce.8
where the time goes:
time: 334 us
  waiting for transfers between devices  202 us (60%)
  matrix products  42 us (13%)
  blocking collectives  27.1 us (8%)
  other arithmetic  26.9 us (8%)
  local copies, waits for them, and re-layouts  21.1 us (6%)
  between operations  14 us (4%)
    psum x1, waiting for transfers between devices, on_device(): input_grad = lax.psum(partial_rows.astype(jnp.bfloat16), 'tp')  86.5 us
    all_gather x1, waiting for transfers between devices, on_device(): pieces = lax.all_gather(paired, 'fs', axis=1, tiled=True)  80.2 us
    reduce_scatter x1, waiting for transfers between devices, on_device(): lax.psum_scatter(make_term(up_grad).astype(jnp.bfloat16), 'fs', scatter_d...  35.6 us
    psum x1, blocking collectives, on_device(): tap_total, bias_total = lax.psum((tap_local, bias_local), 'fs')  27.1 us
    unnamed x38, local copies, waits for them, and re-layouts  16.1 us
    dot_general x2, matrix products, contract_last(): lax.dot_general(left, right, (((1,), (1,)), ((), ())), preferred_element_...  12.8 us
    dot_general x2, matrix products, contract_first(): lax.dot_general(left, right, (((0,), (0,)), ((), ())), preferred_element_...  10.2 us
    dot_general x1, matrix products, on_device(): jnp.dot(stacked_rows, pieces[1], preferred_element_type=jnp.float32)  10.1 us
  transfers between devices with their start and end apart: 4, of which 3 were waited for; matrix products, arithmetic and copies ran while one was open for 12% of the time, Pallas kernels for 0%

commit v1 on v0

--- a/solution.py
+++ b/solution.py
@@ -91,7 +91,7 @@
     ).astype(jnp.float32)
     pieces = lax.all_gather(paired, "fs", axis=1, tiled=True)
     partial_rows = contract_last(gate_grad, pieces[0]) + contract_last(up_grad, pieces[1])
-    input_grad = lax.psum(partial_rows.astype(jnp.bfloat16), "tp")
+    input_grad = jnp.sum(lax.all_gather(partial_rows.astype(jnp.bfloat16), "tp"), axis=0)
     gate_grad_out = gate_grad_sum + grad_scale * gate_summed
     up_grad_out = up_grad_sum + grad_scale * up_summed
     gate_back = gate_float[1:]

time: 334 us -> 375 us (1.12)
  waiting for transfers between devices: 202 us -> 237 us
  other arithmetic: 26.9 us -> 37.2 us
  local copies, waits for them, and re-layouts: 21.1 us -> 17.1 us
    all_gather x0 -> x1, waiting for transfers between devices: none -> 121 us  [on_device(): lax.all_gather(partial_rows.astype(jnp.bfloat16), 'tp')]
    psum x1 -> x0, waiting for transfers between devices: 86.5 us -> none  [on_device(): input_grad = lax.psum(partial_rows.astype(jnp.bfloat16), 'tp')]
    reduce_sum x0 -> x1, other arithmetic: none -> 10.3 us  [on_device(): jnp.sum(lax.all_gather(partial_rows.astype(jnp.bfloat16), 'tp'), axis=0)]
    unnamed x38 -> x37, local copies, waits for them, and re-layouts: 16.1 us -> 12.2 us
  transfers between devices with their start and end apart: 4 -> 4, of which waited for: 3 -> 3; matrix products, arithmetic and copies ran while one was open for 12% -> 11% of each run, Pallas kernels for 0% -> 0%
where the time goes in v1:
time: 375 us; the launch traced here: 374 us
  waiting for transfers between devices  237 us (63%)
  matrix products  42 us (11%)
  other arithmetic  37.2 us (10%)
  blocking collectives  27.1 us (7%)
  local copies, waits for them, and re-layouts  17.1 us (5%)
  between operations  14 us (4%)
    all_gather x1, waiting for transfers between devices, on_device(): lax.all_gather(partial_rows.astype(jnp.bfloat16), 'tp')  121 us
    all_gather x1, waiting for transfers between devices, on_device(): pieces = lax.all_gather(paired, 'fs', axis=1, tiled=True)  80.2 us
    reduce_scatter x1, waiting for transfers between devices, on_device(): lax.psum_scatter(make_term(up_grad).astype(jnp.bfloat16), 'fs', scatter_d...  35.6 us
    psum x1, blocking collectives, on_device(): tap_total, bias_total = lax.psum((tap_local, bias_local), 'fs')  27.1 us
    dot_general x2, matrix products, contract_last(): lax.dot_general(left, right, (((1,), (1,)), ((), ())), preferred_element_...  12.8 us
    unnamed x37, local copies, waits for them, and re-layouts  12.2 us
    reduce_sum x1, other arithmetic, on_device(): jnp.sum(lax.all_gather(partial_rows.astype(jnp.bfloat16), 'tp'), axis=0)  10.3 us
    dot_general x2, matrix products, contract_first(): lax.dot_general(left, right, (((0,), (0,)), ((), ())), preferred_element_...  10.2 us
  transfers between devices with their start and end apart: 4, of which 3 were waited for; matrix products, arithmetic and copies ran while one was open for 11% of the time, Pallas kernels for 0%

profile of v1, /device:TPU:0, one launch (start us, length us, event | category | flops | bytes accessed | tf_op | source)
XLA Modules:
  0.0 374.4 jit_solution(15005811123654166943)
XLA Ops:
  7.2 0.0 all-gather.4.cloned.1.call-start
  7.2 2.4 pad_maximum_fusion
  9.6 0.0 all-gather.4.cloned.1.call-update
  9.7 0.0 reduce-scatter.3.cloned.1.call-start
  9.7 0.0 copy-start.5
  9.7 0.9 fusion.32
  10.7 2.0 constant_dynamic-update-slice_fusion.1
  12.6 2.1 constant_dynamic-update-slice_fusion
  14.8 80.2 %all-gather.4.cloned.1.call-done = bf16[2,2048,1024]{2,1,0:T(8,128)(2,1)} async-done(((bf16[2,256,1024]{2,1,0:T(8,128)(2,1)}), bf16[2,2048,1024]{2,1,0:T(8,128)(2,1)}) %all-gather.4.cloned.1.call-update) | async-done | bytes 8388624 | tf_op jit(solution)/shard_map/all_gather | solution.py:62
  95.0 10.1 %convolution_convert_fusion = bf16[1536,1024]{1,0:T(8,128)(2,1)S(1)} fusion(bf16[1536,2048]{1,0:T(8,128)(2,1)} %constant_dynamic-update-slice_fusion, bf16[2,2048,1024]{2,1,0:T(8,128)(2,1)} %all-gather.4.cloned.1.call-done), kind=kOutput, calls=%fused_computation.15 | convolution fusion | flops 6444023808 | bytes 13631488 | tf_op jit(solution)/shard_map/dot_general | solution.py:64
  105.1 8.8 %convolution_convert_fusion.1 = bf16[1536,1024]{1,0:T(8,128)(2,1)S(1)} fusion(bf16[1536,2048]{1,0:T(8,128)(2,1)} %constant_dynamic-update-slice_fusion, bf16[2,2048,1024]{2,1,0:T(8,128)(2,1)S(1)} %copy-done.15), kind=kOutput, calls=%fused_computation.16 | convolution fusion | flops 6444023808 | bytes 13631488 | tf_op jit(solution)/shard_map/dot_general | solution.py:63
  113.9 0.7 convert_element_type.61
  114.7 1.9 slice_bitcast_fusion.6
  116.5 0.7 convert_element_type.62
  117.3 3.2 add_divide_fusion
  120.5 0.6 copy-done.1
  121.1 6.3 %fusion.13 = (f32[1024]{0:T(1024)S(1)}, f32[1024]{0:T(1024)S(1)}, f32[1024]{0:T(1024)S(1)}, f32[1024]{0:T(1024)S(1)}, f32[1,768,1024]{2,1,0:T(8,128)S(1)}) fusion(f32[1,768,1024]{2,1,0:T(8,128)} %slice_bitcast_fusion.6, f32[1536,1024]{1,0:T(8,128)S(1)} %convert_element_type.61, f32[2,768,1024]{2,1,0:T(8,128)S(1)} %get-tuple-element.24, ...), kind=kLoop, calls=%fused_computation.29 | loop fusion | flops 11005952 | bytes 20463616 | tf_op jit(solution)/shard_map/reduce_sum | solution.py:100
  127.4 0.0 copy-start.6
  127.4 1.0 fusion.10
  128.4 0.0 copy-start.9
  128.4 1.1 copy-done.9
  129.5 5.1 %convert_bitcast_fusion.1 = bf16[2048,1024]{0,1:T(8,128)(2,1)} fusion(bf16[768,2048]{1,0:T(8,128)(2,1)S(1)} %copy-done.6, bf16[1,768,1024]{2,1,0:T(8,128)(2,1)S(1)} %fusion.10), kind=kOutput, calls=%fused_computation.12 | convolution fusion | flops 3223322624 | bytes 8912896 | tf_op jit(solution)/shard_map/dot_general | solution.py:40
  134.7 0.0 reduce-scatter.3.cloned.1.call-update
  134.7 0.2 reduce-scatter.5.cloned.1.call-start
  134.9 4.5 %fusion.29 = f32[2,768,1024]{2,1,0:T(8,128)S(1)} fusion(f32[2,768,1024]{2,1,0:T(8,128)} %copy-done), kind=kLoop, calls=%fused_computation.55 | loop fusion | flops 6291456 | bytes 12582912 | tf_op jit(solution)/shard_map/mul | solution.py:72
  139.5 2.6 copy-done.2
  142.1 5.1 %convert_bitcast_fusion = bf16[2048,1024]{0,1:T(8,128)(2,1)} fusion(bf16[768,2048]{1,0:T(8,128)(2,1)S(1)} %copy-done.6, f32[2,768,1024]{2,1,0:T(8,128)S(1)} %fusion.29, bf16[768,1024]{1,0:T(8,128)(2,1)S(1)} %copy-done.7), kind=kOutput, calls=%fused_computation.11 | convolution fusion | flops 3225681920 | bytes 12058624 | tf_op jit(solution)/shard_map/dot_general | solution.py:40
  147.2 0.0 reduce-scatter.5.cloned.1.call-update
  147.2 0.0 copy-start.8
  147.2 0.0 all-gather.6.cloned.1.call-start
  147.3 1.3 copy-done.10
  148.6 5.5 %fusion.5 = f32[768,2048]{1,0:T(8,128)S(1)} fusion(bf16[2,2048,1024]{2,1,0:T(8,128)(2,1)} %all-gather.4.cloned.1.call-done, bf16[1,768,1024]{2,1,0:T(8,128)(2,1)S(1)} %copy-done.10), kind=kOutput, calls=%fused_computation.17 | convolution fusion | flops 3221225472 | bytes 12058624 | tf_op jit(solution)/shard_map/dot_general | solution.py:34
  154.1 0.0 copy-start.11
  154.1 7.3 %add_convert_fusion = bf16[768,2048]{1,0:T(8,128)(2,1)} fusion(f32[768,2048]{1,0:T(8,128)S(1)} %fusion.5, bf16[2,2048,1024]{2,1,0:T(8,128)(2,1)} %all-gather.4.cloned.1.call-done, f32[2,768,1024]{2,1,0:T(8,128)S(1)} %copy-done.3, bf16[768,1024]{1,0:T(8,128)(2,1)S(1)} %copy-done.8), kind=kOutput, calls=%fused_computation.7 | convolution fusion | flops 3226730496 | bytes 18350080 | tf_op jit(solution)/shard_map/dot_general | solution.py:34
  161.5 0.0 all-gather.6.cloned.1.call-update
  161.5 0.3 copy.17
  161.8 1.6 copy.18
  163.4 27.1 %all-reduce.6 = (f32[3,1024]{1,0:T(4,128)S(1)}, f32[1024]{0:T(1024)S(1)}) all-reduce(f32[3,1024]{1,0:T(4,128)S(1)} %pad_maximum_fusion.1, f32[1024]{0:T(1024)S(1)} %get-tuple-element.18), channel_id=1, replica_groups=mesh['fs'=8,'tp'=4] {'fs'}, use_global_device_ids=true, to_apply=%region_6.7 | all-reduce | flops 4096 | bytes 32768 | tf_op jit(solution)/shard_map/psum | solution.py:105
  190.6 0.6 multiply_add_fusion.3
  191.2 0.6 multiply_add_fusion.2
  191.8 4.5 %fusion.23 = bf16[768,1024]{1,0:T(8,128)(2,1)} fusion(f32[2,768,1024]{2,1,0:T(8,128)} %bitcast.62, f32[2,768,1024]{2,1,0:T(8,128)} %copy-done.2), kind=kLoop, calls=%fused_computation.43 | loop fusion | flops 1572864 | bytes 7864320 | tf_op jit(solution)/shard_map/squeeze | solution.py:74
  196.3 1.2 multiply_add_fusion.1
  197.5 1.3 copy.19
  198.8 35.6 %reduce-scatter.5.cloned.1.call-done = bf16[256,1024]{0,1:T(8,128)(2,1)} async-done(((bf16[2048,1024]{0,1:T(8,128)(2,1)}), bf16[256,1024]{0,1:T(8,128)(2,1)}) %reduce-scatter.5.cloned.1.call-update) | async-done | bytes 524304 | tf_op jit(solution)/shard_map/reduce_scatter | solution.py:84
  234.4 1.2 multiply_add_fusion
  235.6 1.3 copy.20
  236.9 120.7 %all-gather.6.cloned.1.call-done = bf16[3072,2048]{1,0:T(8,128)(2,1)} async-done(((bf16[768,2048]{1,0:T(8,128)(2,1)}), bf16[3072,2048]{1,0:T(8,128)(2,1)}) %all-gather.6.cloned.1.call-update) | async-done | bytes 12582928 | tf_op jit(solution)/shard_map/all_gather | solution.py:94
  357.5 10.3 %reduce_sum.48 = bf16[768,2048]{1,0:T(8,128)(2,1)} reduce(bf16[4,768,2048]{2,1,0:T(8,128)(2,1)} %bitcast.63, bf16[]{:T(256)} %constant.6.clone.1), dimensions={0}, to_apply=%region_0.1 | reduce | flops 4718592 | bytes 15728642 | tf_op jit(solution)/shard_map/reduce_sum | solution.py:94
  (25 shorter events, 0.1 us)
Async XLA Ops:
  7.2 3.5 copy-start.4
  7.2 87.8 %all-gather.4.cloned.1.call-start = ((), (), s32[]{:S(2)}) async-start(), calls=%async_computation.2 | async-start | bytes 9437184 | tf_op jit(solution)/shard_map/all_gather | solution.py:62
  9.7 186.6 %reduce-scatter.3.cloned.1.call-start = ((), (), s32[]{:S(2)}) async-start(), calls=%async_computation.3 | async-start | bytes 4718592 | tf_op jit(solution)/shard_map/reduce_scatter | solution.py:89
  9.7 2.9 copy-start.5
  95.0 10.1 %copy-start.15 = (bf16[2,2048,1024]{2,1,0:T(8,128)(2,1)S(1)}, bf16[2,2048,1024]{2,1,0:T(8,128)(2,1)}, u32[]{:S(2)}) copy-start(bf16[2,2048,1024]{2,1,0:T(8,128)(2,1)} %all-gather.4.cloned.1.call-done) | copy-start | bytes 25165828
  116.5 0.7 copy-start.14
  117.3 3.8 %copy-start.1 = (f32[1536,1024]{1,0:T(8,128)}, f32[1536,1024]{1,0:T(8,128)S(1)}, u32[]{:S(2)}) copy-start(f32[1536,1024]{1,0:T(8,128)S(1)} %convert_element_type.62) | copy-start | bytes 18874372
  120.5 6.9 %copy-start = (f32[2,768,1024]{2,1,0:T(8,128)}, f32[2,768,1024]{2,1,0:T(8,128)S(1)}, u32[]{:S(2)}) copy-start(f32[2,768,1024]{2,1,0:T(8,128)S(1)} %get-tuple-element.24) | copy-start | bytes 18874372
  127.4 2.2 copy-start.6
  128.4 1.1 copy-start.9
  134.7 99.7 %reduce-scatter.5.cloned.1.call-start = ((), (), s32[]{:S(2)}) async-start(), calls=%async_computation.4 | async-start | bytes 4718592 | tf_op jit(solution)/shard_map/reduce_scatter | solution.py:84
  134.9 7.2 %copy-start.7 = (bf16[768,1024]{1,0:T(8,128)(2,1)S(1)}, bf16[768,1024]{1,0:T(8,128)(2,1)}, u32[]{:S(2)}) copy-start(bf16[768,1024]{1,0:T(8,128)(2,1)} %param.13) | copy-start | bytes 4718596
  139.5 2.6 copy-start.2
  147.2 1.4 copy-start.10
  147.2 6.9 %copy-start.8 = (bf16[768,1024]{1,0:T(8,128)(2,1)S(1)}, bf16[768,1024]{1,0:T(8,128)(2,1)}, u32[]{:S(2)}) copy-start(bf16[768,1024]{1,0:T(8,128)(2,1)} %param.13) | copy-start | bytes 4718596
  147.2 210.3 %all-gather.6.cloned.1.call-start = ((), (), s32[]{:S(2)}) async-start(), calls=%async_computation.5 | async-start | bytes 15728640 | tf_op jit(solution)/shard_map/all_gather | solution.py:94
  148.6 5.5 %copy-start.3 = (f32[2,768,1024]{2,1,0:T(8,128)S(1)}, f32[2,768,1024]{2,1,0:T(8,128)}, u32[]{:S(2)}) copy-start(f32[2,768,1024]{2,1,0:T(8,128)} %copy-done.2) | copy-start | bytes 18874372
  154.1 7.4 %copy-start.11 = (f32[256,1024]{1,0:T(8,128)S(1)}, f32[256,1024]{1,0:T(8,128)}, u32[]{:S(2)}) copy-start(f32[256,1024]{1,0:T(8,128)} %param.18) | copy-start | bytes 3145732
  161.5 29.1 %copy-start.13 = (f32[1024]{0:T(1024)S(1)}, f32[1024]{0:T(1024)}, u32[]{:S(2)}) copy-start(f32[1024]{0:T(1024)} %param.21) | copy-start | bytes 12292
  161.5 29.7 %copy-start.12 = (f32[3,1024]{1,0:T(4,128)S(1)}, f32[3,1024]{1,0:T(4,128)}, u32[]{:S(2)}) copy-start(f32[3,1024]{1,0:T(4,128)} %param.20) | copy-start | bytes 36868
Sparse Core Ops, SparseCore 0:
  10.2 84.7 all-gather.3
  134.8 48.8 reduce-scatter.2
  186.0 48.3 reduce-scatter.4
  236.7 120.8 all-gather.5
